TPU v7x, 512 devices: a whole 4x8x8 slice. The times are simulated.
512 devices in a mesh: sp: 32 (over z, x), dp: 16 (over y, core).
Axes of the slice: x: 4, y: 8, z: 8, core: 2. Of those that a mesh axis runs over, the one named last changes fastest.
Arguments:
- query_rows: bfloat16 [16, 4096, 2048], P('dp', 'sp'), may hold values from -6 to 6
- key_rows: bfloat16 [16, 4096, 2048], P('dp', 'sp'), may hold values from -6 to 6
- value_rows: bfloat16 [16, 4096, 2048], P('dp', 'sp'), may hold values from -6 to 6
- decay_low: bfloat16 [16, 4096, 128], P('dp', 'sp'), may hold values from -5 to 5
- rate_low: bfloat16 [16, 4096, 128], P('dp', 'sp'), may hold values from -4 to 4
- decay_up: bfloat16 [128, 2048], replicated, may hold values from -0.5 to 0.5
- rate_up: bfloat16 [128, 2048], replicated, may hold values from -0.5 to 0.5
- decay_base: float32 [2048], replicated, may hold values from -12 to -2
- norm_gain: float32 [2048], replicated, may hold values from 0.1 to 1.9
- out_weight: bfloat16 [2048, 2048], P(None, 'dp'), may hold values from -0.125 to 0.125
Outputs:
- layer_out: bfloat16 [16, 4096, 2048], P('dp', 'sp')
All inputs are finite; a program needn't handle non-finite values.
Results may differ from a plain program's by a relative error of at most 0.005.
Values may be sent and summed in bfloat16 or wider, within the bound.
No kernel may reach another device: no remote copies, remote signals or barrier semaphores. Data moves between devices by JAX's collectives and lax.ppermute only.
A program may use at most 128 MiB of HBM per device.

v0:
```python
import math
import jax
import jax.numpy as jnp
from jax import lax
from jax.sharding import Mesh
from jax.sharding import PartitionSpec as P

HEAD = 64
DP = ("dp_0", "dp_1")
HIGHEST = lax.Precision.HIGHEST
THREE_PASS = lax.Precision.HIGH


def in_order(pieces, dim):
    lengths = list(pieces.shape[1:])
    lengths[dim] *= pieces.shape[0]
    return jnp.moveaxis(pieces, 0, dim).reshape(lengths)


def gather_in_order(value, axes, turns):
    pieces = value
    for k in turns:
        pieces = lax.all_gather(pieces, axes[k])
    done = turns[::-1]
    back = [done.index(k) for k in range(len(axes))]
    pieces = pieces.transpose(*back, *range(len(axes), pieces.ndim))
    return pieces.reshape(-1, *value.shape)


def gathered_by_axis(value, axes, turns, dim):
    return in_order(gather_in_order(value, axes, turns), dim)


def product(form, left, right):
    return jnp.einsum(form, left, right, precision=HIGHEST)


def product_three(form, left, right):
    return jnp.einsum(form, left, right, precision=THREE_PASS)


def to_blocks(rows, heads, block_len):
    positions = rows.shape[0]
    return rows.reshape(positions // block_len, block_len, heads, -1).transpose(2, 0, 3, 1)


def compose(earlier, later):
    return (
        product("hbij,hbjk->hbik", later[0], earlier[0]),
        product("hbij,hbjk->hbik", later[0], earlier[1]) + later[1],
    )


def pre_gates(low_decay, low_rate, decay_up, rate_up, decay_base):
    squashed = jnp.tanh(low_decay.astype(jnp.float32)).astype(jnp.bfloat16)
    decay_pre = (
        decay_base + jnp.dot(squashed, decay_up, preferred_element_type=jnp.float32)
    ).astype(jnp.bfloat16)
    rate_pre = jnp.dot(low_rate, rate_up, preferred_element_type=jnp.float32).astype(jnp.bfloat16)
    return (decay_pre, rate_pre)


def run_mixer(reads, keyed, valued, decay_in, rate_in, gain_here):
    positions = reads.shape[0]
    heads = reads.shape[1] // HEAD
    block_len = math.gcd(positions, 128)
    middle = block_len // 2
    query_blocks = to_blocks(reads.astype(jnp.float32), heads, block_len)
    key_blocks = to_blocks(keyed.astype(jnp.float32), heads, block_len)
    value_blocks = to_blocks(valued.astype(jnp.float32), heads, block_len)
    log_decay = -jnp.exp(-jax.nn.softplus(-decay_in.astype(jnp.float32)) - 0.5)
    decay_blocks = to_blocks(log_decay, heads, block_len)
    rate_blocks = to_blocks(jax.nn.sigmoid(rate_in.astype(jnp.float32)), heads, block_len)
    unit_keys = key_blocks * lax.rsqrt(
        1.0 + jnp.sum(key_blocks * key_blocks, axis=2, keepdims=True)
    )
    erase = unit_keys * rate_blocks
    row_index = lax.broadcasted_iota(jnp.int32, (block_len, block_len), 0)
    col_index = lax.broadcasted_iota(jnp.int32, (block_len, block_len), 1)
    upper = (row_index <= col_index).astype(jnp.float32)
    running = product("hbnc,cd->hbnd", decay_blocks, upper)
    before = running - decay_blocks
    centre = running[..., middle : middle + 1]
    final = running[..., block_len - 1 :]
    read_mid = query_blocks * jnp.exp(running - centre)
    erase_from = unit_keys * jnp.exp(before - centre)
    key_to = key_blocks * jnp.exp(centre - running)
    erase_to = erase * jnp.exp(centre - running)
    read_start = query_blocks * jnp.exp(running)
    erase_start = unit_keys * jnp.exp(before)
    key_end = key_blocks * jnp.exp(final - running)
    erase_end = erase * jnp.exp(final - running)
    strict = row_index > col_index
    within = row_index >= col_index
    key_pairs = jnp.where(strict, product_three("hbnt,hbns->hbts", erase_from, key_to), 0.0)
    erase_pairs = jnp.where(strict, product("hbnt,hbns->hbts", erase_from, erase_to), 0.0)
    read_keys = jnp.where(within, product_three("hbnt,hbns->hbts", read_mid, key_to), 0.0)
    read_erase = jnp.where(within, product_three("hbnt,hbns->hbts", read_mid, erase_to), 0.0)
    lower_matrix = jnp.eye(block_len, dtype=jnp.float32) + erase_pairs
    carried = product_three("hbts,hbms->hbtm", key_pairs, value_blocks)
    right_sides = jnp.concatenate([jnp.swapaxes(erase_start, 2, 3), carried], axis=-1)
    solved = jax.scipy.linalg.solve_triangular(
        lower_matrix, right_sides, lower=True, unit_diagonal=True
    )
    start_weights = solved[..., :HEAD]
    local_erase = solved[..., HEAD:]
    transfer = jnp.eye(HEAD, dtype=jnp.float32) * jnp.exp(final) - product_three(
        "hbnt,hbtk->hbnk", erase_end, start_weights
    )
    added = product_three("hbnt,hbmt->hbnm", key_end, value_blocks) - product_three(
        "hbnt,hbtm->hbnm", erase_end, local_erase
    )
    _, ends = lax.associative_scan(compose, (transfer, added), axis=1)
    starts = jnp.concatenate([jnp.zeros_like(ends[:, :1]), ends[:, :-1]], axis=1)
    read_state = jnp.swapaxes(read_start, 2, 3) - product_three(
        "hbts,hbsn->hbtn", read_erase, start_weights
    )
    readout = (
        product_three("hbtn,hbnm->hbtm", read_state, starts)
        + product_three("hbts,hbms->hbtm", read_keys, value_blocks)
        - product_three("hbts,hbsm->hbtm", read_erase, local_erase)
    )
    average = jnp.mean(readout, axis=-1, keepdims=True)
    centred = readout - average
    variance = jnp.mean(centred * centred, axis=-1, keepdims=True)
    normed = centred * lax.rsqrt(variance + 1.0)
    rows_out = normed.transpose(1, 2, 0, 3).reshape(positions, heads * HEAD)
    return (rows_out * gain_here).astype(jnp.bfloat16)


def per_device(
    query_rows,
    key_rows,
    value_rows,
    decay_low,
    rate_low,
    decay_up,
    rate_up,
    decay_base,
    norm_gain,
    out_weight,
):
    whole_weight = gathered_by_axis(out_weight, DP, (0, 1), 1)
    reads = query_rows[0]
    keyed = key_rows[0]
    valued = value_rows[0]
    decay_pre, rate_pre = pre_gates(decay_low[0], rate_low[0], decay_up, rate_up, decay_base)
    got_reads, got_keys, got_values, got_decay, got_rate = (
        lax.all_to_all(reads, "sp", split_axis=1, concat_axis=0, tiled=True),
        lax.all_to_all(keyed, "sp", split_axis=1, concat_axis=0, tiled=True),
        lax.all_to_all(valued, "sp", split_axis=1, concat_axis=0, tiled=True),
        lax.all_to_all(decay_pre, "sp", split_axis=1, concat_axis=0, tiled=True),
        lax.all_to_all(rate_pre, "sp", split_axis=1, concat_axis=0, tiled=True),
    )
    width_here = got_reads.shape[1]
    gain_here = lax.dynamic_slice_in_dim(norm_gain, lax.axis_index("sp") * width_here, width_here)
    mix = run_mixer(got_reads, got_keys, got_values, got_decay, got_rate, gain_here)
    back = lax.all_to_all(mix, "sp", split_axis=0, concat_axis=1, tiled=True)
    layer_out = jnp.dot(back, whole_weight, preferred_element_type=jnp.float32).astype(jnp.bfloat16)
    return layer_out[None]


def solution(mesh):
    split = Mesh(mesh.devices.reshape(mesh.shape["sp"], 8, 2), ("sp", "dp_0", "dp_1"))
    placed = (
        P(DP, "sp", None),
        P(DP, "sp", None),
        P(DP, "sp", None),
        P(DP, "sp", None),
        P(DP, "sp", None),
        P(),
        P(),
        P(),
        P(),
        P(None, DP),
    )
    return jax.shard_map(
        per_device, mesh=split, in_specs=placed, out_specs=P(DP, "sp", None), check_vma=False
    )
```

profile of v0, /device:TPU:2, one launch (start us, length us, event | category | flops | bytes accessed | tf_op | source)
XLA Modules:
  0.0 559.0 jit_solution(18431480282763413623)
XLA Ops:
  7.6 1.0 fusion
  9.7 13.5 %all-to-all-start.1 = ((bf16[128,32,64]{0,2,1:T(8,128)(2,1)}), bf16[128,32,64]{0,2,1:T(8,128)(2,1)S(1)}, u32[]{:S(2)}, u32[]{:S(2)}) async-start(bf16[128,32,64]{0,2,1:T(8,128)(2,1)} %bitcast.5), calls=%async_computation.1 | async-start | bytes 1048576 | tf_op jit(solution)/shard_map/all_to_all | solution.py:152
  24.1 15.8 %all-to-all-done.1 = bf16[128,32,64]{0,2,1:T(8,128)(2,1)S(1)} async-done(((bf16[128,32,64]{0,2,1:T(8,128)(2,1)}), bf16[128,32,64]{0,2,1:T(8,128)(2,1)S(1)}, u32[]{:S(2)}, u32[]{:S(2)}) %all-to-all-start.1) | async-done | bytes 524320 | tf_op jit(solution)/shard_map/all_to_all | solution.py:152
  40.0 5.7 %all-to-all-start.2 = ((bf16[128,32,64]{0,2,1:T(8,128)(2,1)}), bf16[128,32,64]{0,2,1:T(8,128)(2,1)S(1)}, u32[]{:S(2)}, u32[]{:S(2)}) async-start(bf16[128,32,64]{0,2,1:T(8,128)(2,1)} %bitcast.18), calls=%async_computation.2 | async-start | bytes 1048576 | tf_op jit(solution)/shard_map/all_to_all | solution.py:150
  46.0 1.0 copy.38
  47.1 14.6 %all-to-all-done.2 = bf16[128,32,64]{0,2,1:T(8,128)(2,1)S(1)} async-done(((bf16[128,32,64]{0,2,1:T(8,128)(2,1)}), bf16[128,32,64]{0,2,1:T(8,128)(2,1)S(1)}, u32[]{:S(2)}, u32[]{:S(2)}) %all-to-all-start.2) | async-done | bytes 524320 | tf_op jit(solution)/shard_map/all_to_all | solution.py:150
  61.6 5.6 all-to-all-start.3
  67.2 1.0 copy.39
  69.3 1.3 dynamic_slice.3
  70.9 1.4 fusion.50
  72.2 10.9 %all-to-all-done.3 = bf16[128,32,64]{0,2,1:T(8,128)(2,1)S(1)} async-done(((bf16[128,32,64]{0,2,1:T(8,128)(2,1)}), bf16[128,32,64]{0,2,1:T(8,128)(2,1)S(1)}, u32[]{:S(2)}, u32[]{:S(2)}) %all-to-all-start.3) | async-done | bytes 524320 | tf_op jit(solution)/shard_map/all_to_all | solution.py:153
  84.0 6.1 %all-to-all-start.4 = ((bf16[128,32,64]{0,2,1:T(8,128)(2,1)}), bf16[128,32,64]{0,2,1:T(8,128)(2,1)S(1)}, u32[]{:S(2)}, u32[]{:S(2)}) async-start(bf16[128,32,64]{0,2,1:T(8,128)(2,1)} %bitcast.37), calls=%async_computation.4 | async-start | bytes 1048576 | tf_op jit(solution)/shard_map/all_to_all | solution.py:151
  90.1 1.4 exponential_reduce_fusion
  91.5 5.9 %add_bitcast_fusion = f32[32,1,128,128]{3,2,1,0:T(8,128)} fusion(f32[128,128]{1,0:T(8,128)S(1)} %fusion.149, f32[128,128]{1,0:T(8,128)S(1)} %get-tuple-element.11, pred[128,128]{1,0:T(8,128)(4,1)S(1)} %iota_compare_fusion.1, pred[128,128]{1,0:T(8,128)(4,1)S(1)} %get-tuple-element.10, bf16[128,32,64]{0,2,1:T(8,128)(2,1)S(1)} %all-to-all-done.2, ...), kind=kOutput, calls=%fused_computation.15 | convolution fusion | flops 411303936 | bytes 4907008 | tf_op jit(solution)/shard_map/hbnt,hbns->hbts/dot_general | solution.py:35
  97.4 315.8 %custom-call.4 = f32[32,1,128,128]{2,3,1,0:T(8,128)} custom-call(f32[32,1,128,128]{3,2,1,0:T(8,128)} %add_bitcast_fusion), custom_call_target="InvertDiagBlocksLowerTriangular" | custom-call | tf_op jit(solution)/shard_map/jit(_solve_triangular)/vmap()/triangular_solve | solution.py:102
  413.2 4.0 fusion.60
  417.1 9.8 %all-to-all-start = ((bf16[128,32,64]{0,2,1:T(8,128)(2,1)}), bf16[128,32,64]{0,2,1:T(8,128)(2,1)S(1)}, u32[]{:S(2)}, u32[]{:S(2)}) async-start(bf16[128,32,64]{0,2,1:T(8,128)(2,1)} %bitcast), calls=%async_computation | async-start | bytes 1048576 | tf_op jit(solution)/shard_map/all_to_all | solution.py:149
  426.9 11.6 %all-gather.7.cloned.1.call-start = ((), (), s32[]{:S(2)}) async-start(), calls=%async_computation.7 | async-start | bytes 12582912 | tf_op jit(solution)/shard_map/all_gather | solution.py:23
  438.6 4.2 fusion.23
  442.7 2.0 fusion.71
  444.7 1.7 fusion.56
  446.4 4.3 fusion.14
  450.8 1.4 fusion.30
  452.3 1.3 fusion.29
  457.7 2.0 pad.34
  460.4 2.1 pad.35
  462.4 1.7 add.150
  464.1 3.5 pad.37
  467.6 1.3 fusion.42
  469.5 1.6 pad.36
  471.1 1.7 add.152
  472.8 1.4 fusion.40
  474.4 5.1 pad.39
  479.5 1.9 add.154
  481.4 9.2 %pad.87 = f32[1,32,64,64]{3,2,1,0:T(8,128)} pad(f32[1,16,64,64]{3,2,1,0:T(8,128)} %add.154, f32[]{:T(128)} %constant.12.clone.1), padding=0_0_0x1_0_1x0_0_0x0_0_0 | pad | bytes 786436
  490.5 1.9 fusion.38
  492.5 5.9 %pad.53 = f32[1,31,64,64]{3,2,1,0:T(8,128)} pad(f32[1,16,64,64]{3,2,1,0:T(8,128)S(1)} %pad_maximum_fusion, f32[]{:T(128)} %constant.12.clone.1), padding=0_0_0x0_0_1x0_0_0x0_0_0 | pad | bytes 770052 | tf_op jit(solution)/shard_map/slice | solution.py:114
  498.4 2.8 slice_add_fusion
  501.2 2.6 fusion.65
  503.9 2.2 fusion.34
  507.1 2.8 fusion.58
  509.9 1.6 fusion.26
  511.5 2.2 fusion.178
  514.0 1.1 multiply_convert_fusion
  515.0 9.9 %all-to-all-start.5 = ((bf16[32,128,64]{1,2,0:T(8,128)(2,1)}), bf16[32,128,64]{1,2,0:T(8,128)(2,1)S(1)}, u32[]{:S(2)}, u32[]{:S(2)}) async-start(bf16[32,128,64]{1,2,0:T(8,128)(2,1)} %multiply_convert_fusion), calls=%async_computation.5 | async-start | bytes 1048576 | tf_op jit(solution)/shard_map/all_to_all | solution.py:158
  525.0 7.4 %copy.42 = bf16[8,2,2048,128]{3,2,1,0:T(8,128)(2,1)} copy(bf16[8,2,2048,128]{3,2,0,1:T(8,128)(2,1)} %bitcast.422) | data formatting | bytes 16777216 | tf_op jit(solution)/shard_map/transpose | solution.py:26
  532.4 12.4 %copy.43 = bf16[2048,16,128]{0,2,1:T(8,128)(2,1)} copy(bf16[2048,16,128]{2,0,1:T(8,128)(2,1)} %bitcast.421) | data formatting | bytes 16777216 | tf_op jit(solution)/shard_map/transpose | solution.py:17
  544.8 7.2 %fusion.1 = bf16[1,128,2048]{2,1,0:T(8,128)(2,1)} fusion(bf16[128,2048]{0,1:T(8,128)(2,1)S(1)} %bitcast.424, bf16[2048,2048]{0,1:T(8,128)(2,1)} %bitcast.420), kind=kOutput, calls=%fused_computation.5 | convolution fusion | flops 1074003968 | bytes 9437184 | tf_op jit(solution)/shard_map/dot_general | solution.py:159
  (96 shorter events, 12.1 us)
Async XLA Ops:
  6.5 1.0 copy-start
  6.5 16.6 %copy-start.10 = (bf16[1,128,2048]{2,1,0:T(8,128)(2,1)S(1)}, bf16[1,128,2048]{2,1,0:T(8,128)(2,1)}, u32[]{:S(2)}) copy-start(bf16[1,128,2048]{2,1,0:T(8,128)(2,1)} %param.11) | copy-start | bytes 1572868
  6.5 439.9 %all-gather.5.cloned.1.call-start = ((), (), s32[]{:S(2)}) async-start(), calls=%async_computation.6 | async-start | bytes 4718592 | tf_op jit(solution)/shard_map/all_gather | solution.py:23
  8.6 37.0 %copy-start.11 = (bf16[128,2048]{1,0:T(8,128)(2,1)S(1)}, bf16[128,2048]{1,0:T(8,128)(2,1)}, u32[]{:S(2)}) copy-start(bf16[128,2048]{1,0:T(8,128)(2,1)} %param.16) | copy-start | bytes 1572868
  8.6 37.0 %copy-start.22 = (bf16[1,128,128]{2,1,0:T(8,128)(2,1)S(1)}, bf16[1,128,128]{2,1,0:T(8,128)(2,1)}, u32[]{:S(2)}) copy-start(bf16[1,128,128]{2,1,0:T(8,128)(2,1)} %param.14) | copy-start | bytes 98308
  9.7 30.3 %all-to-all-start.1 = ((bf16[128,32,64]{0,2,1:T(8,128)(2,1)}), bf16[128,32,64]{0,2,1:T(8,128)(2,1)S(1)}, u32[]{:S(2)}, u32[]{:S(2)}) async-start(bf16[128,32,64]{0,2,1:T(8,128)(2,1)} %bitcast.5), calls=%async_computation.1 | async-start | bytes 1048576 | tf_op jit(solution)/shard_map/all_to_all | solution.py:152
  40.0 27.3 %copy-start.12 = (bf16[1,128,2048]{2,1,0:T(8,128)(2,1)S(1)}, bf16[1,128,2048]{2,1,0:T(8,128)(2,1)}, u32[]{:S(2)}) copy-start(bf16[1,128,2048]{2,1,0:T(8,128)(2,1)} %param.12) | copy-start | bytes 1572868
  40.0 21.7 %all-to-all-start.2 = ((bf16[128,32,64]{0,2,1:T(8,128)(2,1)}), bf16[128,32,64]{0,2,1:T(8,128)(2,1)S(1)}, u32[]{:S(2)}, u32[]{:S(2)}) async-start(bf16[128,32,64]{0,2,1:T(8,128)(2,1)} %bitcast.18), calls=%async_computation.2 | async-start | bytes 1048576 | tf_op jit(solution)/shard_map/all_to_all | solution.py:150
  45.7 22.6 %copy-start.13 = (bf16[1,128,2048]{2,1,0:T(8,128)(2,1)S(1)}, bf16[1,128,2048]{2,1,0:T(8,128)(2,1)}, u32[]{:S(2)}) copy-start(bf16[1,128,2048]{2,1,0:T(8,128)(2,1)} %param.10) | copy-start | bytes 1572868
  61.6 21.5 %all-to-all-start.3 = ((bf16[128,32,64]{0,2,1:T(8,128)(2,1)}), bf16[128,32,64]{0,2,1:T(8,128)(2,1)S(1)}, u32[]{:S(2)}, u32[]{:S(2)}) async-start(bf16[128,32,64]{0,2,1:T(8,128)(2,1)} %bitcast.25), calls=%async_computation.3 | async-start | bytes 1048576 | tf_op jit(solution)/shard_map/all_to_all | solution.py:153
  70.9 381.4 %copy-start.20 = (f32[32,128]{1,0:T(8,128)}, f32[32,128]{1,0:T(8,128)S(1)}, u32[]{:S(2)}) copy-start(f32[32,128]{1,0:T(8,128)S(1)} %add_rsqrt_fusion.1) | copy-start | bytes 49156
  83.2 0.8 copy-start.14
  84.0 333.2 %all-to-all-start.4 = ((bf16[128,32,64]{0,2,1:T(8,128)(2,1)}), bf16[128,32,64]{0,2,1:T(8,128)(2,1)S(1)}, u32[]{:S(2)}, u32[]{:S(2)}) async-start(bf16[128,32,64]{0,2,1:T(8,128)(2,1)} %bitcast.37), calls=%async_computation.4 | async-start | bytes 1048576 | tf_op jit(solution)/shard_map/all_to_all | solution.py:151
  90.1 1.5 copy-start.15
  91.5 321.7 %copy-start.18 = (f32[32,64]{1,0:T(8,128)}, f32[32,64]{1,0:T(8,128)S(1)}, u32[]{:S(2)}) copy-start(f32[32,64]{1,0:T(8,128)S(1)} %get-tuple-element.7) | copy-start | bytes 24580
  417.1 84.0 %all-to-all-start = ((bf16[128,32,64]{0,2,1:T(8,128)(2,1)}), bf16[128,32,64]{0,2,1:T(8,128)(2,1)S(1)}, u32[]{:S(2)}, u32[]{:S(2)}) async-start(bf16[128,32,64]{0,2,1:T(8,128)(2,1)} %bitcast), calls=%async_computation | async-start | bytes 1048576 | tf_op jit(solution)/shard_map/all_to_all | solution.py:149
  426.9 98.0 %all-gather.7.cloned.1.call-start = ((), (), s32[]{:S(2)}) async-start(), calls=%async_computation.7 | async-start | bytes 12582912 | tf_op jit(solution)/shard_map/all_gather | solution.py:23
  446.4 4.4 copy-start.8
  446.4 4.4 copy-start.16
  450.8 1.5 copy-start.2
  452.3 1.3 copy-start.7
  453.6 2.1 copy-start.4
  454.3 2.2 copy-start.6
  455.3 1.2 copy-start.9
  456.7 12.1 %slice-start.2 = ((f32[1,8,64,64]{3,2,1,0:T(8,128)}), f32[1,1,64,64]{3,2,1,0:T(8,128)S(1)}, s32[]{:S(2)}) async-start(f32[1,8,64,64]{3,2,1,0:T(8,128)} %copy-done.9), calls=%async_computation.10 | async-start | bytes 65536 | tf_op jit(solution)/shard_map/slice | solution.py:113
  459.7 14.5 %slice-start = ((f32[1,16,64,64]{3,2,1,0:T(8,128)}), f32[1,1,64,64]{3,2,1,0:T(8,128)S(1)}, s32[]{:S(2)}) async-start(f32[1,16,64,64]{3,2,1,0:T(8,128)} %copy-done.6), calls=%async_computation.8 | async-start | bytes 65536 | tf_op jit(solution)/shard_map/slice | solution.py:113
  481.4 11.1 %slice-start.1 = ((f32[1,32,64,64]{3,2,1,0:T(8,128)}), f32[1,1,64,64]{3,2,1,0:T(8,128)S(1)}, s32[]{:S(2)}) async-start(f32[1,32,64,64]{3,2,1,0:T(8,128)} %copy-done.7), calls=%async_computation.9 | async-start | bytes 65536 | tf_op jit(solution)/shard_map/slice | solution.py:113
  492.5 8.7 %copy-start.19 = (f32[32,64]{1,0:T(8,128)S(1)}, f32[32,64]{1,0:T(8,128)}, u32[]{:S(2)}) copy-start(f32[32,64]{1,0:T(8,128)} %copy-done.18) | copy-start | bytes 24580
  492.5 8.6 %copy-start.21 = (f32[32,128]{1,0:T(8,128)S(1)}, f32[32,128]{1,0:T(8,128)}, u32[]{:S(2)}) copy-start(f32[32,128]{1,0:T(8,128)} %copy-done.20) | copy-start | bytes 49156
  498.4 2.8 copy-start.17
  501.2 2.7 copy-start.3
  503.9 2.3 copy-start.5
  511.5 2.4 copy-start.23
  515.0 29.7 %all-to-all-start.5 = ((bf16[32,128,64]{1,2,0:T(8,128)(2,1)}), bf16[32,128,64]{1,2,0:T(8,128)(2,1)S(1)}, u32[]{:S(2)}, u32[]{:S(2)}) async-start(bf16[32,128,64]{1,2,0:T(8,128)(2,1)} %multiply_convert_fusion), calls=%async_computation.5 | async-start | bytes 1048576 | tf_op jit(solution)/shard_map/all_to_all | solution.py:158
  544.8 7.2 %copy-start.1 = (bf16[128,2048]{1,0:T(8,128)(2,1)S(1)}, bf16[128,2048]{1,0:T(8,128)(2,1)}, u32[]{:S(2)}) copy-start(bf16[128,2048]{1,0:T(8,128)(2,1)} %param.15) | copy-start | bytes 1572868
Sparse Core Ops, SparseCore 0:
  9.4 61.7 all-gather.4
  446.5 28.9 all-gather.6
where the time goes:
time: 566 us; the launch traced here: 559 us
  other arithmetic  329 us (58%)
  starting transfers between devices  62.1 us (11%)
  local copies, waits for them, and re-layouts  58.2 us (10%)
  matrix products  53 us (9%)
  waiting for transfers between devices  42.1 us (7%)
  between operations  14.3 us (3%)
    another operation x4, other arithmetic, run_mixer(): jax.scipy.linalg.solve_triangular(lower_matrix, right_sides, lower=True,...  316 us
    dot_general x11, matrix products, product_three(): return jnp.einsum(form, left, right, precision=THREE_PASS)  25 us
    all_to_all x1, waiting for transfers between devices, per_device(): lax.all_to_all(decay_pre, 'sp', split_axis=1, concat_axis=0, tiled=True)  15.8 us
    dot_general x15, matrix products, product(): return jnp.einsum(form, left, right, precision=HIGHEST)  15.2 us
    all_to_all x1, waiting for transfers between devices, per_device(): lax.all_to_all(keyed, 'sp', split_axis=1, concat_axis=0, tiled=True)  14.6 us
    pad x6, local copies, waits for them, and re-layouts, run_mixer(): _, ends = lax.associative_scan(compose, (transfer, added), axis=1)  14.3 us
    all_to_all x1, starting transfers between devices, per_device(): lax.all_to_all(decay_pre, 'sp', split_axis=1, concat_axis=0, tiled=True)  13.5 us
    unnamed x52, local copies, waits for them, and re-layouts  13.4 us
  transfers between devices with their start and end apart: 8, of which 3 were waited for; matrix products, arithmetic and copies ran while one was open for 77% of the time, Pallas kernels for 0%

commit v1 on v0

--- a/solution.py
+++ b/solution.py
@@ -149,7 +149,12 @@
         lax.all_to_all(reads, "sp", split_axis=1, concat_axis=0, tiled=True),
         lax.all_to_all(keyed, "sp", split_axis=1, concat_axis=0, tiled=True),
         lax.all_to_all(valued, "sp", split_axis=1, concat_axis=0, tiled=True),
-        lax.all_to_all(decay_pre, "sp", split_axis=1, concat_axis=0, tiled=True),
+        jnp.concatenate(
+            lax.all_to_all(
+                jnp.stack(jnp.split(decay_pre, lax.axis_size("sp"), axis=1)), "sp", 0, 0
+            ),
+            axis=0,
+        ),
         lax.all_to_all(rate_pre, "sp", split_axis=1, concat_axis=0, tiled=True),
     )
     width_here = got_reads.shape[1]

time: 566 us -> 558 us (0.986)
  the two profiles are of different devices: /device:TPU:2 before, /device:TPU:26 now
where the time goes in v1:
time: 558 us; the launch traced here: 550 us
  other arithmetic  329 us (59%)
  local copies, waits for them, and re-layouts  60.2 us (11%)
  matrix products  53.2 us (10%)
  starting transfers between devices  50.6 us (9%)
  waiting for transfers between devices  42.1 us (8%)
  between operations  14.5 us (3%)
    another operation x4, other arithmetic, run_mixer(): jax.scipy.linalg.solve_triangular(lower_matrix, right_sides, lower=True,...  316 us
    dot_general x11, matrix products, product_three(): return jnp.einsum(form, left, right, precision=THREE_PASS)  25.2 us
    all_to_all x1, waiting for transfers between devices, per_device(): lax.all_to_all(jnp.stack(jnp.split(decay_pre, lax.axis_size('sp'), axis=1...  15.8 us
    dot_general x15, matrix products, product(): return jnp.einsum(form, left, right, precision=HIGHEST)  15.2 us
    unnamed x83, local copies, waits for them, and re-layouts  15.1 us
    all_to_all x1, waiting for transfers between devices, per_device(): lax.all_to_all(keyed, 'sp', split_axis=1, concat_axis=0, tiled=True)  14.6 us
    pad x6, local copies, waits for them, and re-layouts, run_mixer(): _, ends = lax.associative_scan(compose, (transfer, added), axis=1)  14.3 us
    all_to_all x1, starting transfers between devices, per_device(): lax.all_to_all(jnp.stack(jnp.split(decay_pre, lax.axis_size('sp'), axis=1...  13.5 us
  transfers between devices with their start and end apart: 8, of which 3 were waited for; matrix products, arithmetic and copies ran while one was open for 79% of the time, Pallas kernels for 0%

profile of v1, /device:TPU:26, one launch (start us, length us, event | category | flops | bytes accessed | tf_op | source)
XLA Modules:
  0.0 549.8 jit_solution(1613645323860984914)
XLA Ops:
  7.6 1.0 fusion
  10.6 1.1 copy.100
  11.7 13.5 %all-to-all-start.1 = ((bf16[32,128,64]{1,2,0:T(8,128)(2,1)}), bf16[32,128,64]{1,2,0:T(8,128)(2,1)S(1)}, u32[]{:S(2)}, u32[]{:S(2)}) async-start(bf16[32,128,64]{1,2,0:T(8,128)(2,1)} %copy.100), calls=%async_computation.1 | async-start | bytes 1048576 | tf_op jit(solution)/shard_map/all_to_all | solution.py:153
  26.2 15.8 %all-to-all-done.1 = bf16[32,128,64]{1,2,0:T(8,128)(2,1)S(1)} async-done(((bf16[32,128,64]{1,2,0:T(8,128)(2,1)}), bf16[32,128,64]{1,2,0:T(8,128)(2,1)S(1)}, u32[]{:S(2)}, u32[]{:S(2)}) %all-to-all-start.1) | async-done | bytes 524320 | tf_op jit(solution)/shard_map/all_to_all | solution.py:153
  42.0 5.7 %all-to-all-start.2 = ((bf16[128,32,64]{0,2,1:T(8,128)(2,1)}), bf16[128,32,64]{0,2,1:T(8,128)(2,1)S(1)}, u32[]{:S(2)}, u32[]{:S(2)}) async-start(bf16[128,32,64]{0,2,1:T(8,128)(2,1)} %bitcast.48), calls=%async_computation.2 | async-start | bytes 1048576 | tf_op jit(solution)/shard_map/all_to_all | solution.py:150
  48.1 1.0 copy.102
  49.2 14.6 %all-to-all-done.2 = bf16[128,32,64]{0,2,1:T(8,128)(2,1)S(1)} async-done(((bf16[128,32,64]{0,2,1:T(8,128)(2,1)}), bf16[128,32,64]{0,2,1:T(8,128)(2,1)S(1)}, u32[]{:S(2)}, u32[]{:S(2)}) %all-to-all-start.2) | async-done | bytes 524320 | tf_op jit(solution)/shard_map/all_to_all | solution.py:150
  63.7 5.6 %all-to-all-start.3 = ((bf16[128,32,64]{0,2,1:T(8,128)(2,1)}), bf16[128,32,64]{0,2,1:T(8,128)(2,1)S(1)}, u32[]{:S(2)}, u32[]{:S(2)}) async-start(bf16[128,32,64]{0,2,1:T(8,128)(2,1)} %bitcast.55), calls=%async_computation.3 | async-start | bytes 1048576 | tf_op jit(solution)/shard_map/all_to_all | solution.py:158
  70.3 1.0 copy.103
  71.3 1.3 dynamic_slice.3
  72.9 1.4 fusion.50
  74.3 10.9 %all-to-all-done.3 = bf16[128,32,64]{0,2,1:T(8,128)(2,1)S(1)} async-done(((bf16[128,32,64]{0,2,1:T(8,128)(2,1)}), bf16[128,32,64]{0,2,1:T(8,128)(2,1)S(1)}, u32[]{:S(2)}, u32[]{:S(2)}) %all-to-all-start.3) | async-done | bytes 524320 | tf_op jit(solution)/shard_map/all_to_all | solution.py:158
  86.1 6.1 %all-to-all-start.4 = ((bf16[128,32,64]{0,2,1:T(8,128)(2,1)}), bf16[128,32,64]{0,2,1:T(8,128)(2,1)S(1)}, u32[]{:S(2)}, u32[]{:S(2)}) async-start(bf16[128,32,64]{0,2,1:T(8,128)(2,1)} %bitcast.67), calls=%async_computation.4 | async-start | bytes 1048576 | tf_op jit(solution)/shard_map/all_to_all | solution.py:151
  92.2 1.4 exponential_reduce_fusion
  93.7 5.9 %add_bitcast_fusion = f32[32,1,128,128]{3,2,1,0:T(8,128)} fusion(f32[128,128]{1,0:T(8,128)S(1)} %fusion.145, f32[128,128]{1,0:T(8,128)S(1)} %get-tuple-element.11, pred[128,128]{1,0:T(8,128)(4,1)S(1)} %iota_compare_fusion.1, pred[128,128]{1,0:T(8,128)(4,1)S(1)} %get-tuple-element.10, bf16[128,32,64]{0,2,1:T(8,128)(2,1)S(1)} %all-to-all-done.2, ...), kind=kOutput, calls=%fused_computation.15 | convolution fusion | flops 411303936 | bytes 4907008 | tf_op jit(solution)/shard_map/hbnt,hbns->hbts/dot_general | solution.py:35
  99.6 315.8 %custom-call.4 = f32[32,1,128,128]{2,3,1,0:T(8,128)} custom-call(f32[32,1,128,128]{3,2,1,0:T(8,128)} %add_bitcast_fusion), custom_call_target="InvertDiagBlocksLowerTriangular" | custom-call | tf_op jit(solution)/shard_map/jit(_solve_triangular)/vmap()/triangular_solve | solution.py:102
  415.4 4.0 fusion.60
  419.3 9.8 %all-to-all-start = ((bf16[128,32,64]{0,2,1:T(8,128)(2,1)}), bf16[128,32,64]{0,2,1:T(8,128)(2,1)S(1)}, u32[]{:S(2)}, u32[]{:S(2)}) async-start(bf16[128,32,64]{0,2,1:T(8,128)(2,1)} %bitcast), calls=%async_computation | async-start | bytes 1048576 | tf_op jit(solution)/shard_map/all_to_all | solution.py:149
  429.1 4.2 fusion.23
  433.3 2.0 fusion.71
  435.3 1.7 fusion.56
  437.0 4.3 fusion.14
  441.4 1.6 fusion.30
  443.0 1.3 fusion.29
  448.4 2.0 pad.34
  451.1 2.1 pad.35
  453.2 1.7 add.150
  454.9 3.5 pad.37
  458.3 1.3 fusion.42
  460.3 1.6 pad.36
  461.9 1.7 add.152
  463.6 1.4 fusion.40
  465.1 5.1 pad.39
  470.2 1.9 add.154
  472.1 9.2 %pad.87 = f32[1,32,64,64]{3,2,1,0:T(8,128)} pad(f32[1,16,64,64]{3,2,1,0:T(8,128)} %add.154, f32[]{:T(128)} %constant.12.clone.1), padding=0_0_0x1_0_1x0_0_0x0_0_0 | pad | bytes 786436
  481.3 1.9 fusion.38
  483.3 5.9 %pad.53 = f32[1,31,64,64]{3,2,1,0:T(8,128)} pad(f32[1,16,64,64]{3,2,1,0:T(8,128)S(1)} %pad_maximum_fusion, f32[]{:T(128)} %constant.12.clone.1), padding=0_0_0x0_0_1x0_0_0x0_0_0 | pad | bytes 770052 | tf_op jit(solution)/shard_map/slice | solution.py:114
  489.2 2.8 slice_add_fusion
  491.9 2.6 fusion.65
  494.6 2.2 fusion.34
  497.9 2.8 fusion.58
  500.7 1.6 fusion.26
  502.3 2.2 fusion.174
  504.7 1.1 multiply_convert_fusion
  505.8 9.9 %all-to-all-start.5 = ((bf16[32,128,64]{1,2,0:T(8,128)(2,1)}), bf16[32,128,64]{1,2,0:T(8,128)(2,1)S(1)}, u32[]{:S(2)}, u32[]{:S(2)}) async-start(bf16[32,128,64]{1,2,0:T(8,128)(2,1)} %multiply_convert_fusion), calls=%async_computation.5 | async-start | bytes 1048576 | tf_op jit(solution)/shard_map/all_to_all | solution.py:163
  515.7 7.4 %copy.106 = bf16[8,2,2048,128]{3,2,1,0:T(8,128)(2,1)} copy(bf16[8,2,2048,128]{3,2,0,1:T(8,128)(2,1)} %bitcast.520) | data formatting | bytes 16777216 | tf_op jit(solution)/shard_map/transpose | solution.py:26
  523.2 12.4 %copy.107 = bf16[2048,16,128]{0,2,1:T(8,128)(2,1)} copy(bf16[2048,16,128]{2,0,1:T(8,128)(2,1)} %bitcast.519) | data formatting | bytes 16777216 | tf_op jit(solution)/shard_map/transpose | solution.py:17
  535.5 7.2 %fusion.1 = bf16[1,128,2048]{2,1,0:T(8,128)(2,1)} fusion(bf16[128,2048]{0,1:T(8,128)(2,1)S(1)} %bitcast.522, bf16[2048,2048]{0,1:T(8,128)(2,1)} %bitcast.518), kind=kOutput, calls=%fused_computation.5 | convolution fusion | flops 1074003968 | bytes 9437184 | tf_op jit(solution)/shard_map/dot_general | solution.py:164
  (128 shorter events, 13.0 us)
Async XLA Ops:
  6.5 1.0 copy-start
  6.5 430.4 %all-gather.5.cloned.1.call-start = ((), (), s32[]{:S(2)}) async-start(), calls=%async_computation.6 | async-start | bytes 4718592 | tf_op jit(solution)/shard_map/all_gather | solution.py:23
  9.1 16.1 %copy-start.10 = (bf16[1,128,2048]{2,1,0:T(8,128)(2,1)S(1)}, bf16[1,128,2048]{2,1,0:T(8,128)(2,1)}, u32[]{:S(2)}) copy-start(bf16[1,128,2048]{2,1,0:T(8,128)(2,1)} %param.11) | copy-start | bytes 1572868
  10.6 37.2 %copy-start.11 = (bf16[128,2048]{1,0:T(8,128)(2,1)S(1)}, bf16[128,2048]{1,0:T(8,128)(2,1)}, u32[]{:S(2)}) copy-start(bf16[128,2048]{1,0:T(8,128)(2,1)} %param.16) | copy-start | bytes 1572868
  10.6 37.2 %copy-start.22 = (bf16[1,128,128]{2,1,0:T(8,128)(2,1)S(1)}, bf16[1,128,128]{2,1,0:T(8,128)(2,1)}, u32[]{:S(2)}) copy-start(bf16[1,128,128]{2,1,0:T(8,128)(2,1)} %param.14) | copy-start | bytes 98308
  11.7 30.3 %all-to-all-start.1 = ((bf16[32,128,64]{1,2,0:T(8,128)(2,1)}), bf16[32,128,64]{1,2,0:T(8,128)(2,1)S(1)}, u32[]{:S(2)}, u32[]{:S(2)}) async-start(bf16[32,128,64]{1,2,0:T(8,128)(2,1)} %copy.100), calls=%async_computation.1 | async-start | bytes 1048576 | tf_op jit(solution)/shard_map/all_to_all | solution.py:153
  42.0 27.3 %copy-start.12 = (bf16[1,128,2048]{2,1,0:T(8,128)(2,1)S(1)}, bf16[1,128,2048]{2,1,0:T(8,128)(2,1)}, u32[]{:S(2)}) copy-start(bf16[1,128,2048]{2,1,0:T(8,128)(2,1)} %param.10) | copy-start | bytes 1572868
  42.0 21.7 %all-to-all-start.2 = ((bf16[128,32,64]{0,2,1:T(8,128)(2,1)}), bf16[128,32,64]{0,2,1:T(8,128)(2,1)S(1)}, u32[]{:S(2)}, u32[]{:S(2)}) async-start(bf16[128,32,64]{0,2,1:T(8,128)(2,1)} %bitcast.48), calls=%async_computation.2 | async-start | bytes 1048576 | tf_op jit(solution)/shard_map/all_to_all | solution.py:150
  47.8 22.6 %copy-start.13 = (bf16[1,128,2048]{2,1,0:T(8,128)(2,1)S(1)}, bf16[1,128,2048]{2,1,0:T(8,128)(2,1)}, u32[]{:S(2)}) copy-start(bf16[1,128,2048]{2,1,0:T(8,128)(2,1)} %param.12) | copy-start | bytes 1572868
  63.7 21.5 %all-to-all-start.3 = ((bf16[128,32,64]{0,2,1:T(8,128)(2,1)}), bf16[128,32,64]{0,2,1:T(8,128)(2,1)S(1)}, u32[]{:S(2)}, u32[]{:S(2)}) async-start(bf16[128,32,64]{0,2,1:T(8,128)(2,1)} %bitcast.55), calls=%async_computation.3 | async-start | bytes 1048576 | tf_op jit(solution)/shard_map/all_to_all | solution.py:158
  72.9 370.1 %copy-start.20 = (f32[32,128]{1,0:T(8,128)}, f32[32,128]{1,0:T(8,128)S(1)}, u32[]{:S(2)}) copy-start(f32[32,128]{1,0:T(8,128)S(1)} %add_rsqrt_fusion.1) | copy-start | bytes 49156
  85.3 0.8 copy-start.14
  86.1 333.2 %all-to-all-start.4 = ((bf16[128,32,64]{0,2,1:T(8,128)(2,1)}), bf16[128,32,64]{0,2,1:T(8,128)(2,1)S(1)}, u32[]{:S(2)}, u32[]{:S(2)}) async-start(bf16[128,32,64]{0,2,1:T(8,128)(2,1)} %bitcast.67), calls=%async_computation.4 | async-start | bytes 1048576 | tf_op jit(solution)/shard_map/all_to_all | solution.py:151
  92.2 1.5 copy-start.15
  93.7 321.7 %copy-start.18 = (f32[32,64]{1,0:T(8,128)}, f32[32,64]{1,0:T(8,128)S(1)}, u32[]{:S(2)}) copy-start(f32[32,64]{1,0:T(8,128)S(1)} %get-tuple-element.7) | copy-start | bytes 24580
  419.3 72.6 %all-to-all-start = ((bf16[128,32,64]{0,2,1:T(8,128)(2,1)}), bf16[128,32,64]{0,2,1:T(8,128)(2,1)S(1)}, u32[]{:S(2)}, u32[]{:S(2)}) async-start(bf16[128,32,64]{0,2,1:T(8,128)(2,1)} %bitcast), calls=%async_computation | async-start | bytes 1048576 | tf_op jit(solution)/shard_map/all_to_all | solution.py:149
  429.1 86.6 %all-gather.7.cloned.1.call-start = ((), (), s32[]{:S(2)}) async-start(), calls=%async_computation.7 | async-start | bytes 12582912 | tf_op jit(solution)/shard_map/all_gather | solution.py:23
  437.0 4.4 copy-start.8
  437.0 4.4 copy-start.16
  441.4 1.6 copy-start.2
  443.0 1.3 copy-start.7
  444.3 2.1 copy-start.4
  445.0 2.2 copy-start.6
  446.1 1.2 copy-start.9
  447.5 12.1 %slice-start.2 = ((f32[1,8,64,64]{3,2,1,0:T(8,128)}), f32[1,1,64,64]{3,2,1,0:T(8,128)S(1)}, s32[]{:S(2)}) async-start(f32[1,8,64,64]{3,2,1,0:T(8,128)} %copy-done.9), calls=%async_computation.10 | async-start | bytes 65536 | tf_op jit(solution)/shard_map/slice | solution.py:113
  450.5 14.5 %slice-start = ((f32[1,16,64,64]{3,2,1,0:T(8,128)}), f32[1,1,64,64]{3,2,1,0:T(8,128)S(1)}, s32[]{:S(2)}) async-start(f32[1,16,64,64]{3,2,1,0:T(8,128)} %copy-done.6), calls=%async_computation.8 | async-start | bytes 65536 | tf_op jit(solution)/shard_map/slice | solution.py:113
  472.1 11.1 %slice-start.1 = ((f32[1,32,64,64]{3,2,1,0:T(8,128)}), f32[1,1,64,64]{3,2,1,0:T(8,128)S(1)}, s32[]{:S(2)}) async-start(f32[1,32,64,64]{3,2,1,0:T(8,128)} %copy-done.7), calls=%async_computation.9 | async-start | bytes 65536 | tf_op jit(solution)/shard_map/slice | solution.py:113
  483.3 8.7 %copy-start.19 = (f32[32,64]{1,0:T(8,128)S(1)}, f32[32,64]{1,0:T(8,128)}, u32[]{:S(2)}) copy-start(f32[32,64]{1,0:T(8,128)} %copy-done.18) | copy-start | bytes 24580
  483.3 8.6 %copy-start.21 = (f32[32,128]{1,0:T(8,128)S(1)}, f32[32,128]{1,0:T(8,128)}, u32[]{:S(2)}) copy-start(f32[32,128]{1,0:T(8,128)} %copy-done.20) | copy-start | bytes 49156
  489.2 2.8 copy-start.17
  491.9 2.7 copy-start.3
  494.6 2.3 copy-start.5
  502.3 2.4 copy-start.23
  505.8 29.7 %all-to-all-start.5 = ((bf16[32,128,64]{1,2,0:T(8,128)(2,1)}), bf16[32,128,64]{1,2,0:T(8,128)(2,1)S(1)}, u32[]{:S(2)}, u32[]{:S(2)}) async-start(bf16[32,128,64]{1,2,0:T(8,128)(2,1)} %multiply_convert_fusion), calls=%async_computation.5 | async-start | bytes 1048576 | tf_op jit(solution)/shard_map/all_to_all | solution.py:163
  535.5 7.2 %copy-start.1 = (bf16[128,2048]{1,0:T(8,128)(2,1)S(1)}, bf16[128,2048]{1,0:T(8,128)(2,1)}, u32[]{:S(2)}) copy-start(bf16[128,2048]{1,0:T(8,128)(2,1)} %param.15) | copy-start | bytes 1572868
Sparse Core Ops, SparseCore 0:
  9.4 61.2 all-gather.4
  437.1 28.6 all-gather.6
